TPU v7x, 32 devices: a whole 2x2x4 slice. The times are simulated.
32 devices in a mesh: ep: 4 (over y, x), tp: 8 (over z, core).
Axes of the slice: x: 2, y: 2, z: 4, core: 2. Of those that a mesh axis runs over, the one named last changes fastest.
Arguments:
- tokens: bfloat16 [1024, 1024], P(('ep', 'tp')), may hold values from -6 to 6
- norm_gain: float32 [1024], replicated, may hold values from 0.5 to 1.5
- routing: int32 [1024, 2], P('ep'), may hold values from 0 to 7, as said below
- gate_share: float32 [1024, 2], P('ep'), may hold values from 0.5 to 1.5
- w_gate: bfloat16 [8, 1024, 256], P('ep', None, 'tp'), may hold values from -0.1875 to 0.1875
- w_up: bfloat16 [8, 1024, 256], P('ep', None, 'tp'), may hold values from -0.1875 to 0.1875
- w_down: bfloat16 [8, 256, 1024], P('ep', 'tp'), may hold values from -0.375 to 0.375
Outputs:
- mixed_out: bfloat16 [1024, 1024], P('ep', 'tp')
Inputs may be any that keep to these rules, and one draw needn't show every extreme that they name: `routing`: each row names two different experts whose ids lie in the same block of 2 consecutive ids. In each aligned block of 256 rows (the tokens of one index of ep) no expert is named by more than 128 rows, and some expert is named by exactly 128.
All inputs are finite; a program needn't handle non-finite values.
Results may differ from a plain program's by a relative error of at most 0.0015.
Values may be sent and summed in bfloat16 or wider, within the bound.
A program may use at most 64 MiB of HBM per device.

v0:
```python
import jax
import jax.numpy as jnp
from jax import lax
from jax.sharding import PartitionSpec as P

epsilon = 1e-06


def norm_rows(tokens, norm_gain):
    as_float = tokens.astype(jnp.float32)
    scaled = as_float * lax.rsqrt(jnp.mean(as_float * as_float, axis=-1, keepdims=True) + epsilon)
    return (scaled * norm_gain.astype(jnp.float32)).astype(jnp.bfloat16)


def fill_buffer(group, flat_target, slots, model_width):
    buffer = jnp.zeros((slots, model_width), jnp.bfloat16)
    return buffer.at[flat_target].set(jnp.repeat(group, 2, axis=0))


def body(tokens, norm_gain, routing, gate_share, w_gate, w_up, w_down):
    ep_size = lax.axis_size("ep")
    tp_size = lax.axis_size("tp")
    local_experts = w_gate.shape[0]
    experts = local_experts * ep_size
    group_rows = routing.shape[0]
    capacity = group_rows * 4 // experts
    model_width = tokens.shape[1]
    columns = model_width // tp_size
    normed = norm_rows(tokens, norm_gain)
    onehot = (routing[:, :, None] == jnp.arange(experts, dtype=jnp.int32)[None, None, :]).astype(
        jnp.int32
    )
    flat_hot = onehot.reshape(group_rows * 2, experts)
    ranking = jnp.cumsum(flat_hot, axis=0) - 1
    slot_pos = jnp.sum(ranking * flat_hot, axis=1).reshape(group_rows, 2)
    target = (routing * capacity + slot_pos).astype(jnp.int32)
    flat_target = target.reshape(-1)
    slice_len = capacity // tp_size
    tp_index = lax.axis_index("tp")
    group = lax.all_gather(normed, "tp", axis=0, tiled=True)
    buffer = fill_buffer(group, flat_target, experts * capacity, model_width)
    shaped = buffer.reshape(ep_size, local_experts, capacity, model_width)
    mine = lax.dynamic_slice_in_dim(shaped, tp_index * slice_len, slice_len, 2)
    mine = mine.reshape(ep_size, local_experts * slice_len, model_width)
    landed = lax.all_to_all(mine, "ep", split_axis=0, concat_axis=0, tiled=True)
    landed = landed.reshape(ep_size, local_experts, slice_len, model_width).transpose(1, 0, 2, 3)
    landed = landed.reshape(local_experts, ep_size * slice_len, model_width)
    full_gate, full_up, full_down = (
        lax.all_gather(w_gate, "tp", axis=2, tiled=True),
        lax.all_gather(w_up, "tp", axis=2, tiled=True),
        lax.all_gather(w_down, "tp", axis=1, tiled=True),
    )
    gate_sum = jnp.einsum("erd,edh->erh", landed, full_gate, preferred_element_type=jnp.float32)
    up_sum = jnp.einsum("erd,edh->erh", landed, full_up, preferred_element_type=jnp.float32)
    hidden = (jax.nn.silu(gate_sum) * up_sum).astype(jnp.bfloat16)
    produced = jnp.einsum(
        "erh,ehd->erd", hidden, full_down, preferred_element_type=jnp.float32
    ).astype(jnp.bfloat16)
    produced = produced.reshape(local_experts, ep_size, slice_len, model_width)
    blocks = lax.all_to_all(produced, "tp", split_axis=3, concat_axis=2, tiled=True)
    leaving = blocks.transpose(1, 0, 2, 3).reshape(ep_size, local_experts * capacity, columns)
    returned = lax.all_to_all(leaving, "ep", split_axis=0, concat_axis=0, tiled=True).reshape(
        experts * capacity, columns
    )
    picked_out = returned[target]
    mixed_out = jnp.sum(gate_share[:, :, None] * picked_out.astype(jnp.float32), axis=1)
    return mixed_out.astype(jnp.bfloat16)


def solution(mesh):
    return jax.shard_map(
        body,
        mesh=mesh,
        in_specs=(
            P(("ep", "tp"), None),
            P(),
            P("ep", None),
            P("ep", None),
            P("ep", None, "tp"),
            P("ep", None, "tp"),
            P("ep", "tp", None),
        ),
        out_specs=P("ep", "tp"),
        check_vma=False,
    )
```

profile of v0, /device:TPU:0, one launch (start us, length us, event | category | flops | bytes accessed | tf_op | source)
XLA Modules:
  0.0 124.9 jit_solution(3098279486913121579)
XLA Ops:
  6.5 0.0 all-gather.4.cloned.1.call-start
  6.5 0.7 all-gather.4.cloned.1.call-update
  7.3 0.0 all-gather.6.cloned.1.call-start
  7.3 0.7 all-gather.6.cloned.1.call-update
  8.0 0.0 all-gather.8.cloned.1.call-start
  8.1 0.7 all-gather.8.cloned.1.call-update
  8.7 0.8 copy.34
  9.6 0.1 eq.30
  9.7 0.1 eq.26
  9.9 1.1 reduce-window.6
  11.0 0.2 slice_reduce_fusion
  11.3 0.1 fusion.13
  11.4 0.1 reshape.89
  11.5 0.1 copy.36
  11.6 0.7 compare_select_fusion.1
  12.3 0.1 copy.37
  12.4 0.2 reshape.90
  12.6 1.0 fusion.4
  13.6 0.9 fusion.6
  14.5 19.1 %all_gather.12 = bf16[256,1024]{1,0:T(8,128)(2,1)S(1)} all-gather(bf16[32,1024]{1,0:T(8,128)(2,1)S(1)} %fusion.6), channel_id=1, replica_groups=mesh['ep'=4,'tp'=8] {'tp'}, dimensions={0}, use_global_device_ids=true | all-gather | bytes 589824 | tf_op jit(solution)/shard_map/all_gather | solution.py:40
  33.6 0.5 broadcast_in_dim.7
  34.1 0.4 reshape.111
  34.6 3.2 %scatter_custom_fusion = bf16[1024,1024]{1,0:T(8,128)(2,1)S(1)} fusion(s32[512]{0:T(512)S(1)} %bitcast.42, bf16[512,1024]{1,0:T(8,128)(2,1)S(1)} %reshape.111, bf16[]{:T(256)} %constant.11.clone.1), kind=kCustom, calls=%fused_computation.5 | custom fusion | bytes 2097154 | tf_op jit(solution)/shard_map/scatter | solution.py:17
  37.9 9.8 %all_to_all.28 = bf16[4,32,1024]{2,1,0:T(8,128)(2,1)S(1)} all-to-all(bf16[4,32,1024]{2,1,0:T(8,128)(2,1)S(1)} %bitcast.38), channel_id=1, replica_groups=mesh['ep'=4,'tp'=8] {'ep'}, dimensions={0} | all-to-all | bytes 524288 | tf_op jit(solution)/shard_map/all_to_all | solution.py:45
  47.7 0.0 all-gather.4.cloned.1.call-done
  47.7 1.7 %fusion.16 = f32[2,64,256]{2,1,0:T(8,128)S(1)} fusion(bf16[2,64,1024]{2,1,0:T(8,128)(2,1)S(1)} %bitcast.36, bf16[2,1024,256]{1,2,0:T(8,128)(2,1)} %all-gather.4.cloned.1.call-done), kind=kOutput, calls=%fused_computation.33 | convolution fusion | flops 67108864 | bytes 1441792 | tf_op jit(solution)/shard_map/erd,edh->erh/dot_general | solution.py:53
  49.4 11.1 %all-gather.6.cloned.1.call-done = bf16[2,1024,256]{1,2,0:T(8,128)(2,1)} async-done(((bf16[2,1024,32]{1,2,0:T(8,128)(2,1)}), bf16[2,1024,256]{1,2,0:T(8,128)(2,1)}) %all-gather.6.cloned.1.call-update) | async-done | bytes 1048592 | tf_op jit(solution)/shard_map/all_gather | solution.py:50
  60.5 23.8 %all-gather.8.cloned.1.call-done = bf16[2,256,1024]{2,1,0:T(8,128)(2,1)} async-done(((bf16[2,32,1024]{2,1,0:T(8,128)(2,1)}), bf16[2,256,1024]{2,1,0:T(8,128)(2,1)}) %all-gather.8.cloned.1.call-update) | async-done | bytes 1048592 | tf_op jit(solution)/shard_map/all_gather | solution.py:51
  84.3 2.2 %convolution_convert_fusion = bf16[2,64,1024]{2,1,0:T(8,128)(2,1)S(1)} fusion(bf16[2,256,1024]{2,1,0:T(8,128)(2,1)} %all-gather.8.cloned.1.call-done, bf16[2,64,1024]{2,1,0:T(8,128)(2,1)S(1)} %bitcast.37, bf16[2,1024,256]{1,2,0:T(8,128)(2,1)} %all-gather.6.cloned.1.call-done, f32[2,64,256]{2,1,0:T(8,128)S(1)} %fusion.16), kind=kOutput, calls=%fused_computation.2 | convolution fusion | flops 134545408 | bytes 2752512 | tf_op jit(solution)/shard_map/erh,ehd->erd/dot_general | solution.py:56
  86.5 1.4 %copy.39 = bf16[2,4,16,1024]{2,1,0,3:T(4,128)(2,1)S(1)} copy(bf16[2,4,16,1024]{3,2,1,0:T(8,128)(2,1)S(1)} %bitcast.40) | data formatting | bytes 524288 | tf_op jit(solution)/shard_map/reshape | solution.py:59
  87.9 2.2 %reshape.121 = bf16[8,2,8192]{2,1,0:T(2,128)(2,1)S(1)} reshape(bf16[1024,2,4,16]{3,2,1,0:T(4,128)(2,1)S(1)} %bitcast.32) | data formatting | bytes 524288
  90.1 13.1 %all_to_all.29 = bf16[8,2,8192]{2,1,0:T(2,128)(2,1)S(1)} all-to-all(bf16[8,2,8192]{2,1,0:T(2,128)(2,1)S(1)} %reshape.121), channel_id=1, replica_groups=mesh['ep'=4,'tp'=8] {'tp'}, dimensions={0} | all-to-all | bytes 524288 | tf_op jit(solution)/shard_map/all_to_all | solution.py:60
  103.1 1.4 %reshape.122 = bf16[1024,2,4,16]{3,2,1,0:T(4,128)(2,1)S(1)} reshape(bf16[8,2,8192]{2,1,0:T(2,128)(2,1)S(1)} %all_to_all.29) | data formatting | bytes 524288
  104.6 0.0 copy-start
  104.6 2.6 %copy.46 = bf16[2,4,16,8,128]{4,2,3,0,1:T(8,128)(2,1)} copy(bf16[2,4,16,8,128]{2,1,0,4,3:T(4,128)(2,1)S(1)} %bitcast.33) | data formatting | bytes 524288 | tf_op jit(solution)/shard_map/transpose | solution.py:61
  107.2 3.5 %all-to-all-start.2 = ((bf16[4,256,128]{2,1,0:T(8,128)(2,1)}), bf16[4,256,128]{2,1,0:T(8,128)(2,1)S(1)}, u32[]{:S(2)}, u32[]{:S(2)}) async-start(bf16[4,256,128]{2,1,0:T(8,128)(2,1)} %bitcast.15), calls=%async_computation.2 | async-start | bytes 524288 | tf_op jit(solution)/shard_map/all_to_all | solution.py:62
  110.6 0.1 copy.43
  110.8 0.1 reshape.101
  110.9 0.0 copy-done
  110.9 0.1 copy.33
  111.1 4.9 %all-to-all-done.2 = bf16[4,256,128]{2,1,0:T(8,128)(2,1)S(1)} async-done(((bf16[4,256,128]{2,1,0:T(8,128)(2,1)}), bf16[4,256,128]{2,1,0:T(8,128)(2,1)S(1)}, u32[]{:S(2)}, u32[]{:S(2)}) %all-to-all-start.2) | async-done | bytes 262176 | tf_op jit(solution)/shard_map/all_to_all | solution.py:62
  116.0 1.3 %gather_fusion = bf16[512,128]{1,0:T(8,128)(2,1)S(1)} fusion(bf16[1024,128]{1,0:T(8,128)(2,1)S(1)} %bitcast.34, s32[1024]{0:T(1024)S(1)} %pad_clamp_fusion), kind=kCustom, calls=%fused_computation | custom fusion | bytes 264192 | tf_op jit(solution)/shard_map/gather | solution.py:65
  117.3 1.1 fusion.3
  (8 shorter events, 0.1 us)
Async XLA Ops:
  6.5 41.2 %all-gather.4.cloned.1.call-start = ((), (), s32[]{:S(2)}) async-start(), calls=%async_computation.3 | async-start | bytes 1179648 | tf_op jit(solution)/shard_map/all_gather | solution.py:49
  7.3 53.2 %all-gather.6.cloned.1.call-start = ((), (), s32[]{:S(2)}) async-start(), calls=%async_computation.4 | async-start | bytes 1179648 | tf_op jit(solution)/shard_map/all_gather | solution.py:50
  8.0 76.3 %all-gather.8.cloned.1.call-start = ((), (), s32[]{:S(2)}) async-start(), calls=%async_computation.5 | async-start | bytes 1179648 | tf_op jit(solution)/shard_map/all_gather | solution.py:51
  104.6 6.3 %copy-start = (f32[256,2]{0,1:T(2,128)S(1)}, f32[256,2]{0,1:T(2,128)}, u32[]{:S(2)}) copy-start(f32[256,2]{0,1:T(2,128)} %param.10) | copy-start | bytes 6148
  107.2 8.9 %all-to-all-start.2 = ((bf16[4,256,128]{2,1,0:T(8,128)(2,1)}), bf16[4,256,128]{2,1,0:T(8,128)(2,1)S(1)}, u32[]{:S(2)}, u32[]{:S(2)}) async-start(bf16[4,256,128]{2,1,0:T(8,128)(2,1)} %bitcast.15), calls=%async_computation.2 | async-start | bytes 524288 | tf_op jit(solution)/shard_map/all_to_all | solution.py:62
Sparse Core Ops, SparseCore 0:
  8.9 27.9 all-gather.3
  38.5 21.9 all-gather.5
  62.1 22.1 all-gather.7
where the time goes:
time: 125 us
  waiting for transfers between devices  42 us (34%)
  blocking collectives  41.9 us (34%)
  local copies, waits for them, and re-layouts  15.3 us (12%)
  between operations  13.3 us (11%)
  other arithmetic  4.95 us (4%)
  matrix products  3.89 us (3%)
  starting transfers between devices  3.56 us (3%)
    all_gather x1, waiting for transfers between devices, body(): lax.all_gather(w_down, 'tp', axis=1, tiled=True)  23.8 us
    all_gather x1, blocking collectives, body(): group = lax.all_gather(normed, 'tp', axis=0, tiled=True)  19.1 us
    all_to_all x1, blocking collectives, body(): lax.all_to_all(produced, 'tp', split_axis=3, concat_axis=2, tiled=True)  13.1 us
    all_gather x1, waiting for transfers between devices, body(): lax.all_gather(w_up, 'tp', axis=2, tiled=True)  11.1 us
    all_to_all x1, blocking collectives, body(): landed = lax.all_to_all(mine, 'ep', split_axis=0, concat_axis=0, tiled=True)  9.79 us
    all_to_all x1, waiting for transfers between devices, body(): lax.all_to_all(leaving, 'ep', split_axis=0, concat_axis=0, tiled=True)  4.92 us
    unnamed x6, local copies, waits for them, and re-layouts  4.55 us
    all_to_all x1, starting transfers between devices, body(): lax.all_to_all(leaving, 'ep', split_axis=0, concat_axis=0, tiled=True)  3.48 us
  transfers between devices with their start and end apart: 4, of which 3 were waited for; matrix products, arithmetic and copies ran while one was open for 10% of the time, Pallas kernels for 0%

commit v1 on v0

--- a/solution.py
+++ b/solution.py
@@ -1,9 +1,233 @@
+import functools
+
 import jax
 import jax.numpy as jnp
 from jax import lax
+from jax.experimental import pallas as pl
+from jax.experimental.pallas import tpu as pltpu
 from jax.sharding import PartitionSpec as P
 
 epsilon = 1e-06
+MESH = pl.DeviceIdType.MESH
+CHUNKS = 2
+
+
+def kernel(ep_size, tp_size, cap, tok, gain, routing, share, wg, wu, wd, out,
+           G, OH, OHT, XS, X, H, RS, RET, WC, WDR, BW,
+           s1s, s1r, f1s, f1r, wds, wdr, x2s, x2r, xfs, xfr,
+           h3s, h3r, hfs, hfr, r4s, r4r):
+    g = lax.axis_index("ep")
+    j = lax.axis_index("tp")
+    Z = tp_size // 2
+    z = j // 2
+    core = j % 2
+    partner = z * 2 + (1 - core)
+    rows, D = tok.shape
+    W = D // CHUNKS
+    R2 = cap // 2
+    hs = wg.shape[2]
+    side = ep_size // 2
+
+    def zpeer(k):
+        return ((z + k) % Z) * 2 + core
+
+    def zfrom(k):
+        return (z + Z - k) % Z
+
+    def epeer(d):
+        return ((g // side + d // side) % side) * side + (g % side + d % side) % side
+
+    def rc(src, dst, ss, rs, dev):
+        return pltpu.make_async_remote_copy(src_ref=src, dst_ref=dst, send_sem=ss,
+                                            recv_sem=rs, device_id=dev, device_id_type=MESH)
+
+    sends = []
+
+    def start(cp):
+        cp.start()
+        sends.append(cp)
+
+    bar = pltpu.get_barrier_semaphore()
+    for k in range(1, tp_size):
+        pl.semaphore_signal(bar, inc=1, device_id=(g, (j + k) % tp_size), device_id_type=MESH)
+    for d in range(1, ep_size):
+        pl.semaphore_signal(bar, inc=1, device_id=(epeer(d), j), device_id_type=MESH)
+
+    x = tok[...].astype(jnp.float32)
+    normed = x * lax.rsqrt(jnp.mean(x * x, axis=-1, keepdims=True) + epsilon)
+    normed = (normed * gain[...]).astype(jnp.bfloat16)
+
+    def gblock(c, t):
+        return G.at[c, pl.ds(pl.multiple_of(t * rows, rows), rows), :]
+
+    for c in range(CHUNKS):
+        G[c, pl.ds(pl.multiple_of(j * rows, rows), rows), :] = normed[:, c * W:(c + 1) * W]
+
+    pl.semaphore_wait(bar, tp_size - 1 + ep_size - 1)
+
+    zorder = [Z // 2] + [k for k in range(1, Z) if k != Z // 2]
+    for c in range(CHUNKS):
+        for k in zorder:
+            start(rc(gblock(c, j), gblock(c, j), s1s.at[c, k], s1r.at[c, k], (g, zpeer(k))))
+        start(rc(gblock(c, j), gblock(c, j), s1s.at[c, 0], s1r.at[c, 0], (g, partner)))
+    cols = D // tp_size
+    for k in range(1, tp_size):
+        dst = (j + k) % tp_size
+        start(rc(wd.at[:, :, pl.ds(pl.multiple_of(dst * cols, cols), cols)], WDR.at[j],
+                 wds.at[k], wdr.at[k], (g, dst)))
+    WDR[j] = wd[:, :, pl.ds(pl.multiple_of(j * cols, cols), cols)]
+
+    n = routing.shape[0]
+    local = wg.shape[0]
+    rel = jnp.bitwise_xor(lax.div(routing[:, 0:1], jnp.int32(local)), g)
+    hot = (lax.broadcasted_iota(jnp.int32, (n, 128), 1) == rel)
+    low = lax.broadcasted_iota(jnp.int32, (n, n), 1) < lax.broadcasted_iota(jnp.int32, (n, n), 0)
+    rank = jnp.dot(low.astype(jnp.bfloat16), hot.astype(jnp.bfloat16),
+                   preferred_element_type=jnp.float32)
+    pos = jnp.sum(jnp.where(hot, rank, 0.0), axis=1, keepdims=True)
+    slot = rel.astype(jnp.float32) * cap + pos
+    slots = ep_size * cap
+    OHT[...] = (lax.broadcasted_iota(jnp.int32, (n, slots), 1).astype(jnp.float32)
+                == slot).astype(jnp.bfloat16)
+    slot_row = jnp.transpose(jnp.broadcast_to(slot, (n, 128)))[0:1, :]
+    OH[...] = (lax.broadcasted_iota(jnp.int32, (slots, n), 0).astype(jnp.float32)
+               == slot_row).astype(jnp.bfloat16)
+    for e in range(2):
+        WC[:, e * hs:(e + 1) * hs] = wg[e]
+        WC[:, (2 + e) * hs:(3 + e) * hs] = wu[e]
+    BW[...] = jnp.zeros_like(BW)
+
+    half = pl.multiple_of(core * R2, R2)
+    other = pl.multiple_of((1 - core) * R2, R2)
+    eorder = [ep_size - 1] + list(range(1, ep_size - 1))
+
+    for c in range(CHUNKS):
+        for k in [0] + list(range(1, Z)):
+            if k == 0:
+                src = gblock(c, partner)
+                rc(src, src, s1s.at[c, 0], s1r.at[c, 0], (g, partner)).wait_recv()
+            else:
+                src = gblock(c, zfrom(k) * 2 + core)
+                rc(src, src, s1s.at[c, k], s1r.at[c, k], (g, zpeer(k))).wait_recv()
+                start(rc(src, src, f1s.at[c, k], f1r.at[c, k], (g, partner)))
+        for k in range(1, Z):
+            src = gblock(c, zfrom(k) * 2 + 1 - core)
+            rc(src, src, f1s.at[c, k], f1r.at[c, k], (g, partner)).wait_recv()
+        for d in eorder:
+            oh = OH[pl.ds(pl.multiple_of(d * cap + core * R2, R2), R2), :]
+            XS[c, d] = jnp.dot(oh, G[c], preferred_element_type=jnp.float32).astype(jnp.bfloat16)
+            start(rc(XS.at[c, d], X.at[c, d, pl.ds(half, R2), :], x2s.at[c, d], x2r.at[c, d],
+                     (epeer(d), j)))
+        X[c, 0] = jnp.dot(OH[0:cap, :], G[c], preferred_element_type=jnp.float32).astype(jnp.bfloat16)
+
+    def hblock(d, t):
+        return H.at[d, :, pl.ds(pl.multiple_of(t * 128, 128), 128)]
+
+    def gate_up(d):
+        acc = jnp.dot(X[0, d], WC[0:W, :], preferred_element_type=jnp.float32)
+        for c in range(1, CHUNKS):
+            acc += jnp.dot(X[c, d], WC[c * W:(c + 1) * W, :], preferred_element_type=jnp.float32)
+        gs = acc[:, :2 * hs]
+        us = acc[:, 2 * hs:]
+        hid = gs / (1.0 + jnp.exp(-gs)) * us
+        hid = jnp.concatenate([hid[:R2], hid[R2:]], axis=1).astype(jnp.bfloat16)
+        H[d, :, pl.ds(pl.multiple_of(j * 128, 128), 128)] = hid
+        for k in zorder:
+            start(rc(hblock(d, j), hblock(d, j), h3s.at[d, k], h3r.at[d, k], (g, zpeer(k))))
+        start(rc(hblock(d, j), hblock(d, j), h3s.at[d, 0], h3r.at[d, 0], (g, partner)))
+
+    gate_up(0)
+    earrive = list(range(1, ep_size))
+    for c in range(CHUNKS):
+        for d in earrive:
+            land = X.at[c, d, pl.ds(half, R2), :]
+            rc(land, land, x2s.at[c, d], x2r.at[c, d], (epeer(d), j)).wait_recv()
+            start(rc(land, land, xfs.at[c, d], xfr.at[c, d], (g, partner)))
+    for k in range(1, tp_size):
+        src = (j + tp_size - k) % tp_size
+        rc(WDR.at[src], WDR.at[src], wds.at[k], wdr.at[k], (g, src)).wait_recv()
+    for t in range(tp_size):
+        for q in range(4):
+            BW[t * 128 + q * hs:t * 128 + (q + 1) * hs, q * cols:(q + 1) * cols] = WDR[t, q % 2]
+    for d in earrive:
+        for c in range(CHUNKS):
+            land = X.at[c, d, pl.ds(other, R2), :]
+            rc(land, land, xfs.at[c, d], xfr.at[c, d], (g, partner)).wait_recv()
+        gate_up(d)
+
+    dorder = [0] + earrive
+    for d in dorder:
+        for k in [0] + list(range(1, Z)):
+            if k == 0:
+                src = hblock(d, partner)
+                rc(src, src, h3s.at[d, 0], h3r.at[d, 0], (g, partner)).wait_recv()
+            else:
+                src = hblock(d, zfrom(k) * 2 + core)
+                rc(src, src, h3s.at[d, k], h3r.at[d, k], (g, zpeer(k))).wait_recv()
+                start(rc(src, src, hfs.at[d, k], hfr.at[d, k], (g, partner)))
+    for d in earrive + [0]:
+        for k in range(1, Z):
+            src = hblock(d, zfrom(k) * 2 + 1 - core)
+            rc(src, src, hfs.at[d, k], hfr.at[d, k], (g, partner)).wait_recv()
+        res = jnp.dot(H[d], BW[...], preferred_element_type=jnp.float32).astype(jnp.bfloat16)
+        if d == 0:
+            RET[0, 0:R2, :] = res[:, :2 * cols]
+            RET[0, R2:, :] = res[:, 2 * cols:]
+        else:
+            RS[d, 0:R2, :] = res[:, :2 * cols]
+            RS[d, R2:, :] = res[:, 2 * cols:]
+            start(rc(RS.at[d], RET.at[d], r4s.at[d], r4r.at[d], (epeer(d), j)))
+
+    first = lax.rem(routing[:, 0:1], jnp.int32(local)) == 0
+    s0 = jnp.where(first, share[:, 0:1], share[:, 1:2])
+    s1 = jnp.where(first, share[:, 1:2], share[:, 0:1])
+    total = jnp.dot(OHT[:, 0:cap], RET[0], preferred_element_type=jnp.float32)
+    for d in earrive:
+        rc(RS.at[d], RET.at[d], r4s.at[d], r4r.at[d], (epeer(d), j)).wait_recv()
+        total += jnp.dot(OHT[:, d * cap:(d + 1) * cap], RET[d], preferred_element_type=jnp.float32)
+    out[...] = (s0 * total[:, :cols] + s1 * total[:, cols:]).astype(out.dtype)
+    for cp in sends:
+        cp.wait_send()
+
+
+def fused_body(ep_size, tp_size, tokens, norm_gain, routing, gate_share, w_gate, w_up, w_down):
+    rows, D = tokens.shape
+    local, _, hs = w_gate.shape
+    n = routing.shape[0]
+    cap = n * 4 // (local * ep_size)
+    cols = D // tp_size
+    W = D // CHUNKS
+    Z = tp_size // 2
+    R2 = cap // 2
+    bf = jnp.bfloat16
+    dma = pltpu.SemaphoreType.DMA
+    vm = pltpu.VMEM
+    return pl.pallas_call(
+        functools.partial(kernel, ep_size, tp_size, cap),
+        out_shape=jax.ShapeDtypeStruct((n, cols), bf),
+        in_specs=[pl.BlockSpec(memory_space=pltpu.VMEM)] * 7,
+        out_specs=pl.BlockSpec(memory_space=pltpu.VMEM),
+        scratch_shapes=[
+            vm((CHUNKS, n, W), bf),
+            vm((ep_size * cap, n), bf),
+            vm((n, ep_size * cap), bf),
+            vm((CHUNKS, ep_size, R2, W), bf),
+            vm((CHUNKS, ep_size, cap, W), bf),
+            vm((ep_size, R2, tp_size * 128), bf),
+            vm((ep_size, cap, 2 * cols), bf),
+            vm((ep_size, cap, 2 * cols), bf),
+            vm((D, 4 * hs), bf),
+            vm((tp_size, local, hs, cols), bf),
+            vm((tp_size * 4 * hs, 4 * cols), bf),
+            dma((CHUNKS, Z)), dma((CHUNKS, Z)), dma((CHUNKS, Z)), dma((CHUNKS, Z)),
+            dma((tp_size,)), dma((tp_size,)),
+            dma((CHUNKS, ep_size)), dma((CHUNKS, ep_size)),
+            dma((CHUNKS, ep_size)), dma((CHUNKS, ep_size)),
+            dma((ep_size, Z)), dma((ep_size, Z)), dma((ep_size, Z)), dma((ep_size, Z)),
+            dma((ep_size,)), dma((ep_size,)),
+        ],
+        compiler_params=pltpu.CompilerParams(collective_id=0, has_side_effects=True),
+    )(tokens, norm_gain.reshape(1, D), routing, gate_share, w_gate, w_up, w_down)
 
 
 def norm_rows(tokens, norm_gain):
@@ -68,8 +292,16 @@
 
 
 def solution(mesh):
+    ep_size, tp_size = mesh.shape["ep"], mesh.shape["tp"]
+
+    def either(*arrays):
+        local, _, hs = arrays[4].shape
+        if ep_size == 4 and local == 2 and tp_size % 2 == 0 and 4 * hs == 128:
+            return fused_body(ep_size, tp_size, *arrays)
+        return body(*arrays)
+
     return jax.shard_map(
-        body,
+        either,
         mesh=mesh,
         in_specs=(
             P(("ep", "tp"), None),

time: 125 us -> 43.5 us (0.35)
  waiting for transfers between devices: 42 us -> 0 us
  blocking collectives: 41.9 us -> 0 us
  Pallas kernels: 0 us -> 37.5 us
  between operations: 13.3 us -> 0.01 us
  local copies, waits for them, and re-layouts: 15.3 us -> 5.8 us
  other arithmetic: 4.95 us -> 0 us
  matrix products: 3.89 us -> 0 us
  starting transfers between devices: 3.56 us -> 0 us
    pallas_call x0 -> x1, Pallas kernels: none -> 37.5 us  [fused_body(): pl.pallas_call(functools.partial(kernel, ep_size, tp_size, cap), out_shap...]
    all_gather x3 -> x0, waiting for transfers between devices: 34.9 us -> none  [the longest x1 23.8 us: body(): lax.all_gather(w_down, 'tp', axis=1, tiled=True)]
    all_to_all x2 -> x0, blocking collectives: 22.8 us -> none  [the longest x1 13.1 us: body(): lax.all_to_all(produced, 'tp', split_axis=3, concat_axis=2, tiled=True)]
    all_gather x1 -> x0, blocking collectives: 19.1 us -> none  [body(): group = lax.all_gather(normed, 'tp', axis=0, tiled=True)]
    all_to_all x1 -> x0, waiting for transfers between devices: 4.92 us -> none  [body(): lax.all_to_all(leaving, 'ep', split_axis=0, concat_axis=0, tiled=True)]
    dot_general x2 -> x0, matrix products: 3.89 us -> none  [the longest x1 2.23 us: body(): jnp.einsum('erh,ehd->erd', hidden, full_down, preferred_element_type=jnp....]
    all_to_all x1 -> x0, starting transfers between devices: 3.48 us -> none  [body(): lax.all_to_all(leaving, 'ep', split_axis=0, concat_axis=0, tiled=True)]
    scatter x1 -> x0, local copies, waits for them, and re-layouts: 3.23 us -> none  [fill_buffer(): return buffer.at[flat_target].set(jnp.repeat(group, 2, axis=0))]
  transfers between devices with their start and end apart: 4 -> 0, of which waited for: 3 -> 0; matrix products, arithmetic and copies ran while one was open for 10% -> 0% of each run, Pallas kernels for 0% -> 0%
where the time goes in v1:
time: 43.5 us; the launch traced here: 43.4 us
  Pallas kernels  37.5 us (86%)
  local copies, waits for them, and re-layouts  5.8 us (13%)
    pallas_call x1, Pallas kernels, fused_body(): pl.pallas_call(functools.partial(kernel, ep_size, tp_size, cap), out_shap...  37.5 us
    unnamed x11, local copies, waits for them, and re-layouts  5.8 us

profile of v1, /device:TPU:0, one launch (start us, length us, event | category | flops | bytes accessed | tf_op | source)
XLA Modules:
  0.0 43.4 jit_solution(11896287651187655384)
XLA Ops:
  0.0 0.0 copy-start.2
  0.0 0.0 copy-start
  0.0 1.5 %copy.8.routing = s32[256,2]{1,0:T(8,128)} copy(s32[256,2]{0,1:T(2,128)} %param.9) | data formatting | bytes 4096 | tf_op args[2]
  1.5 0.0 copy-done.2
  1.5 0.8 %copy.9.share = f32[256,2]{1,0:T(8,128)} copy(f32[256,2]{0,1:T(2,128)S(1)} %copy-done.2) | data formatting | bytes 4096 | tf_op args[3]
  2.3 0.0 copy-done
  2.3 0.0 copy-start.1
  2.3 1.0 %copy.10.wg = bf16[2,1024,32]{2,1,0:T(8,128)(2,1)} copy(bf16[2,1024,32]{1,2,0:T(8,128)(2,1)S(1)} %copy-done) | data formatting | bytes 262144 | tf_op args[4]
  3.3 0.0 copy-done.1
  3.3 1.0 %copy.11.wu = bf16[2,1024,32]{2,1,0:T(8,128)(2,1)} copy(bf16[2,1024,32]{1,2,0:T(8,128)(2,1)S(1)} %copy-done.1) | data formatting | bytes 262144 | tf_op args[5]
  4.3 37.5 %shard_map.73 = bf16[256,128]{1,0:T(8,128)(2,1)} custom-call(bf16[32,1024]{1,0:T(8,128)(2,1)} %tok.1, f32[1,1024]{1,0:T(1,128)} %bitcast.1, s32[256,2]{1,0:T(8,128)} %copy.8.routing, f32[256,2]{1,0:T(8,128)} %copy.9.share, bf16[2,1024,32]{2,1,0:T(8,128)(2,1)} %copy.10.wg, bf16[2,1024,32]{2,1,0:T(8,128)(2,1)} %copy.11.wu, bf16[2,32,1024]{2,1,0:T(8,128)(2,1)} %wd.1), custom_call_target="tpu_custom_call" | custom-call | tf_op jit(solution)/shard_map/pallas_call | solution.py:205
  41.9 1.5 %copy.13 = bf16[256,128]{1,0:T(8,128)(2,1)} copy(bf16[256,128]{1,0:T(8,128)(2,1)} %shard_map.73) | data formatting | bytes 131072
Async XLA Ops:
  0.0 1.5 %copy-start.2 = (f32[256,2]{0,1:T(2,128)S(1)}, f32[256,2]{0,1:T(2,128)}, u32[]{:S(2)}) copy-start(f32[256,2]{0,1:T(2,128)} %param.10) | copy-start | bytes 6148
  0.0 2.3 %copy-start = (bf16[2,1024,32]{1,2,0:T(8,128)(2,1)S(1)}, bf16[2,1024,32]{1,2,0:T(8,128)(2,1)}, u32[]{:S(2)}) copy-start(bf16[2,1024,32]{1,2,0:T(8,128)(2,1)} %param.11) | copy-start | bytes 393220
  2.3 1.0 %copy-start.1 = (bf16[2,1024,32]{1,2,0:T(8,128)(2,1)S(1)}, bf16[2,1024,32]{1,2,0:T(8,128)(2,1)}, u32[]{:S(2)}) copy-start(bf16[2,1024,32]{1,2,0:T(8,128)(2,1)} %param.12) | copy-start | bytes 393220

commit v2 on v1

--- a/solution.py
+++ b/solution.py
@@ -9,11 +9,11 @@
 
 epsilon = 1e-06
 MESH = pl.DeviceIdType.MESH
-CHUNKS = 2
-
-
-def kernel(ep_size, tp_size, cap, tok, gain, routing, share, wg, wu, wd, out,
-           G, OH, OHT, XS, X, H, RS, RET, WC, WDR, BW,
+CHUNKS = 4
+
+
+def kernel(ep_size, tp_size, cap, tok_h, gain_h, routing_h, share_h, wg, wu, wd_h, out,
+           tok, gain, routing, share, wd, ins, SHS, SHR, shs, shr, G, OH, OHT, XS, X, H, RS, RET, WC, WDR, BW,
            s1s, s1r, f1s, f1r, wds, wdr, x2s, x2r, xfs, xfr,
            h3s, h3r, hfs, hfr, r4s, r4r):
     g = lax.axis_index("ep")
@@ -22,10 +22,10 @@
     z = j // 2
     core = j % 2
     partner = z * 2 + (1 - core)
-    rows, D = tok.shape
+    rows, D = tok_h.shape
     W = D // CHUNKS
     R2 = cap // 2
-    hs = wg.shape[2]
+    hs = wg.shape[1]
     side = ep_size // 2
 
     def zpeer(k):
@@ -53,6 +53,20 @@
     for d in range(1, ep_size):
         pl.semaphore_signal(bar, inc=1, device_id=(epeer(d), j), device_id_type=MESH)
 
+    def fetch(src, dst, i):
+        cp = pltpu.make_async_copy(src, dst, ins.at[i])
+        cp.start()
+        return cp
+
+    rows_in = [fetch(tok_h, tok, 0), fetch(gain_h, gain, 1)]
+    ids_in = [fetch(routing_h, routing, 2), fetch(share_h, share, 3)]
+    down_in = fetch(wd_h, wd, 4)
+    weights_in = []
+    for e in range(2):
+        weights_in.append(fetch(wg.at[e], WC.at[pl.ds(e * hs, hs), :], 5 + e))
+        weights_in.append(fetch(wu.at[e], WC.at[pl.ds((2 + e) * hs, hs), :], 7 + e))
+    for cp in rows_in:
+        cp.wait()
     x = tok[...].astype(jnp.float32)
     normed = x * lax.rsqrt(jnp.mean(x * x, axis=-1, keepdims=True) + epsilon)
     normed = (normed * gain[...]).astype(jnp.bfloat16)
@@ -71,15 +85,21 @@
             start(rc(gblock(c, j), gblock(c, j), s1s.at[c, k], s1r.at[c, k], (g, zpeer(k))))
         start(rc(gblock(c, j), gblock(c, j), s1s.at[c, 0], s1r.at[c, 0], (g, partner)))
     cols = D // tp_size
-    for k in range(1, tp_size):
-        dst = (j + k) % tp_size
-        start(rc(wd.at[:, :, pl.ds(pl.multiple_of(dst * cols, cols), cols)], WDR.at[j],
-                 wds.at[k], wdr.at[k], (g, dst)))
-    WDR[j] = wd[:, :, pl.ds(pl.multiple_of(j * cols, cols), cols)]
-
-    n = routing.shape[0]
+    for cp in ids_in:
+        cp.wait()
+
+    n = routing.shape[1]
     local = wg.shape[0]
-    rel = jnp.bitwise_xor(lax.div(routing[:, 0:1], jnp.int32(local)), g)
+    rel_row = jnp.bitwise_xor(lax.div(routing[0:1, :], jnp.int32(local)), g)
+    first = lax.rem(routing[0:1, :], jnp.int32(local)) == 0
+    s0_row = jnp.where(first, share[0:1, :], share[1:2, :])
+    s1_row = jnp.where(first, share[1:2, :], share[0:1, :])
+    packed = jnp.concatenate([rel_row.astype(jnp.float32), s0_row, s1_row,
+                              jnp.zeros((125, n), jnp.float32)], axis=0)
+    columns = jnp.transpose(packed)
+    rel = columns[:, 0:1].astype(jnp.int32)
+    s0 = columns[:, 1:2]
+    s1 = columns[:, 2:3]
     hot = (lax.broadcasted_iota(jnp.int32, (n, 128), 1) == rel)
     low = lax.broadcasted_iota(jnp.int32, (n, n), 1) < lax.broadcasted_iota(jnp.int32, (n, n), 0)
     rank = jnp.dot(low.astype(jnp.bfloat16), hot.astype(jnp.bfloat16),
@@ -87,14 +107,20 @@
     pos = jnp.sum(jnp.where(hot, rank, 0.0), axis=1, keepdims=True)
     slot = rel.astype(jnp.float32) * cap + pos
     slots = ep_size * cap
-    OHT[...] = (lax.broadcasted_iota(jnp.int32, (n, slots), 1).astype(jnp.float32)
-                == slot).astype(jnp.bfloat16)
+    mine = lax.broadcasted_iota(jnp.int32, (n, slots), 1).astype(jnp.float32) == slot
+    OHT[...] = mine.astype(jnp.bfloat16)
+    both = jnp.concatenate([jnp.sum(jnp.where(mine, s0, 0.0), axis=0, keepdims=True),
+                            jnp.sum(jnp.where(mine, s1, 0.0), axis=0, keepdims=True),
+                            jnp.zeros((6, slots), jnp.float32)], axis=0)
+    SHR[0] = both[:, 0:cap]
+    for d in range(1, ep_size):
+        SHS[d] = both[:, d * cap:(d + 1) * cap]
+        start(rc(SHS.at[d], SHR.at[d], shs.at[d], shr.at[d], (epeer(d), j)))
     slot_row = jnp.transpose(jnp.broadcast_to(slot, (n, 128)))[0:1, :]
     OH[...] = (lax.broadcasted_iota(jnp.int32, (slots, n), 0).astype(jnp.float32)
                == slot_row).astype(jnp.bfloat16)
-    for e in range(2):
-        WC[:, e * hs:(e + 1) * hs] = wg[e]
-        WC[:, (2 + e) * hs:(3 + e) * hs] = wu[e]
+    for cp in weights_in + [down_in]:
+        cp.wait()
     BW[...] = jnp.zeros_like(BW)
 
     half = pl.multiple_of(core * R2, R2)
@@ -120,13 +146,21 @@
                      (epeer(d), j)))
         X[c, 0] = jnp.dot(OH[0:cap, :], G[c], preferred_element_type=jnp.float32).astype(jnp.bfloat16)
 
+    for k in range(1, tp_size):
+        dst = (j + k) % tp_size
+        start(rc(wd.at[:, :, pl.ds(pl.multiple_of(dst * cols, cols), cols)], WDR.at[j],
+                 wds.at[k], wdr.at[k], (g, dst)))
+    WDR[j] = wd[:, :, pl.ds(pl.multiple_of(j * cols, cols), cols)]
+
     def hblock(d, t):
         return H.at[d, :, pl.ds(pl.multiple_of(t * 128, 128), 128)]
 
     def gate_up(d):
-        acc = jnp.dot(X[0, d], WC[0:W, :], preferred_element_type=jnp.float32)
-        for c in range(1, CHUNKS):
-            acc += jnp.dot(X[c, d], WC[c * W:(c + 1) * W, :], preferred_element_type=jnp.float32)
+        acc = None
+        for c in range(CHUNKS):
+            part = lax.dot_general(X[c, d], WC[:, c * W:(c + 1) * W], (((1,), (1,)), ((), ())),
+                                   preferred_element_type=jnp.float32)
+            acc = part if acc is None else acc + part
         gs = acc[:, :2 * hs]
         us = acc[:, 2 * hs:]
         hid = gs / (1.0 + jnp.exp(-gs)) * us
@@ -136,6 +170,16 @@
             start(rc(hblock(d, j), hblock(d, j), h3s.at[d, k], h3r.at[d, k], (g, zpeer(k))))
         start(rc(hblock(d, j), hblock(d, j), h3s.at[d, 0], h3r.at[d, 0], (g, partner)))
 
+    def take_hidden(d):
+        for k in [0] + list(range(1, Z)):
+            if k == 0:
+                src = hblock(d, partner)
+                rc(src, src, h3s.at[d, 0], h3r.at[d, 0], (g, partner)).wait_recv()
+            else:
+                src = hblock(d, zfrom(k) * 2 + core)
+                rc(src, src, h3s.at[d, k], h3r.at[d, k], (g, zpeer(k))).wait_recv()
+                start(rc(src, src, hfs.at[d, k], hfr.at[d, k], (g, partner)))
+
     gate_up(0)
     earrive = list(range(1, ep_size))
     for c in range(CHUNKS):
@@ -143,6 +187,7 @@
             land = X.at[c, d, pl.ds(half, R2), :]
             rc(land, land, x2s.at[c, d], x2r.at[c, d], (epeer(d), j)).wait_recv()
             start(rc(land, land, xfs.at[c, d], xfr.at[c, d], (g, partner)))
+    take_hidden(0)
     for k in range(1, tp_size):
         src = (j + tp_size - k) % tp_size
         rc(WDR.at[src], WDR.at[src], wds.at[k], wdr.at[k], (g, src)).wait_recv()
@@ -155,37 +200,38 @@
             rc(land, land, xfs.at[c, d], xfr.at[c, d], (g, partner)).wait_recv()
         gate_up(d)
 
-    dorder = [0] + earrive
-    for d in dorder:
-        for k in [0] + list(range(1, Z)):
-            if k == 0:
-                src = hblock(d, partner)
-                rc(src, src, h3s.at[d, 0], h3r.at[d, 0], (g, partner)).wait_recv()
-            else:
-                src = hblock(d, zfrom(k) * 2 + core)
-                rc(src, src, h3s.at[d, k], h3r.at[d, k], (g, zpeer(k))).wait_recv()
-                start(rc(src, src, hfs.at[d, k], hfr.at[d, k], (g, partner)))
-    for d in earrive + [0]:
+    def down(d):
         for k in range(1, Z):
             src = hblock(d, zfrom(k) * 2 + 1 - core)
             rc(src, src, hfs.at[d, k], hfr.at[d, k], (g, partner)).wait_recv()
-        res = jnp.dot(H[d], BW[...], preferred_element_type=jnp.float32).astype(jnp.bfloat16)
-        if d == 0:
-            RET[0, 0:R2, :] = res[:, :2 * cols]
-            RET[0, R2:, :] = res[:, 2 * cols:]
-        else:
-            RS[d, 0:R2, :] = res[:, :2 * cols]
-            RS[d, R2:, :] = res[:, 2 * cols:]
+        res = jnp.dot(H[d], BW[...], preferred_element_type=jnp.float32)
+        res = res.astype(jnp.bfloat16).astype(jnp.float32)
+        a = shares[:, 8 * d:8 * d + 1]
+        b = shares[:, 8 * d + 1:8 * d + 2]
+        target = RET if d == 0 else RS
+        target[d, 0:R2, :] = (a[:R2] * res[:, :cols]
+                              + b[:R2] * res[:, cols:2 * cols]).astype(jnp.bfloat16)
+        target[d, R2:, :] = (a[R2:] * res[:, 2 * cols:3 * cols]
+                             + b[R2:] * res[:, 3 * cols:]).astype(jnp.bfloat16)
+        if d:
             start(rc(RS.at[d], RET.at[d], r4s.at[d], r4r.at[d], (epeer(d), j)))
 
-    first = lax.rem(routing[:, 0:1], jnp.int32(local)) == 0
-    s0 = jnp.where(first, share[:, 0:1], share[:, 1:2])
-    s1 = jnp.where(first, share[:, 1:2], share[:, 0:1])
+    for d in earrive:
+        rc(SHS.at[d], SHR.at[d], shs.at[d], shr.at[d], (epeer(d), j)).wait_recv()
+    shares = jnp.transpose(jnp.concatenate(
+        [SHR[d] for d in range(ep_size)] + [jnp.zeros((128 - 8 * ep_size, cap), jnp.float32)], axis=0))
+    down(0)
+    take_hidden(1)
+    for d in earrive[1:]:
+        take_hidden(d)
+        down(d - 1)
+    down(ep_size - 1)
+
     total = jnp.dot(OHT[:, 0:cap], RET[0], preferred_element_type=jnp.float32)
     for d in earrive:
         rc(RS.at[d], RET.at[d], r4s.at[d], r4r.at[d], (epeer(d), j)).wait_recv()
         total += jnp.dot(OHT[:, d * cap:(d + 1) * cap], RET[d], preferred_element_type=jnp.float32)
-    out[...] = (s0 * total[:, :cols] + s1 * total[:, cols:]).astype(out.dtype)
+    out[...] = total.astype(out.dtype)
     for cp in sends:
         cp.wait_send()
 
@@ -205,18 +251,23 @@
     return pl.pallas_call(
         functools.partial(kernel, ep_size, tp_size, cap),
         out_shape=jax.ShapeDtypeStruct((n, cols), bf),
-        in_specs=[pl.BlockSpec(memory_space=pltpu.VMEM)] * 7,
+        in_specs=[pl.BlockSpec(memory_space=pltpu.HBM)] * 7,
         out_specs=pl.BlockSpec(memory_space=pltpu.VMEM),
         scratch_shapes=[
+            vm((rows, D), bf), vm((1, D), jnp.float32),
+            vm((2, n), jnp.int32), vm((2, n), jnp.float32), vm((local, hs, D), bf),
+            dma((9,)),
+            vm((ep_size, 8, cap), jnp.float32), vm((ep_size, 8, cap), jnp.float32),
+            dma((ep_size,)), dma((ep_size,)),
             vm((CHUNKS, n, W), bf),
             vm((ep_size * cap, n), bf),
             vm((n, ep_size * cap), bf),
             vm((CHUNKS, ep_size, R2, W), bf),
             vm((CHUNKS, ep_size, cap, W), bf),
             vm((ep_size, R2, tp_size * 128), bf),
-            vm((ep_size, cap, 2 * cols), bf),
-            vm((ep_size, cap, 2 * cols), bf),
-            vm((D, 4 * hs), bf),
+            vm((ep_size, cap, cols), bf),
+            vm((ep_size, cap, cols), bf),
+            vm((4 * hs, D), bf),
             vm((tp_size, local, hs, cols), bf),
             vm((tp_size * 4 * hs, 4 * cols), bf),
             dma((CHUNKS, Z)), dma((CHUNKS, Z)), dma((CHUNKS, Z)), dma((CHUNKS, Z)),
@@ -226,8 +277,10 @@
             dma((ep_size, Z)), dma((ep_size, Z)), dma((ep_size, Z)), dma((ep_size, Z)),
             dma((ep_size,)), dma((ep_size,)),
         ],
-        compiler_params=pltpu.CompilerParams(collective_id=0, has_side_effects=True),
-    )(tokens, norm_gain.reshape(1, D), routing, gate_share, w_gate, w_up, w_down)
+        compiler_params=pltpu.CompilerParams(collective_id=0, has_side_effects=True,
+                                             vmem_limit_bytes=67043328),
+    )(tokens, norm_gain.reshape(1, D), routing.T, gate_share.T, w_gate.swapaxes(1, 2),
+      w_up.swapaxes(1, 2), w_down)
 
 
 def norm_rows(tokens, norm_gain):

time: 43.5 us -> 38.6 us (0.89)
  local copies, waits for them, and re-layouts: 5.8 us -> 1.47 us
  Pallas kernels: 37.5 us -> 36.9 us
    unnamed x11 -> x1, local copies, waits for them, and re-layouts: 5.8 us -> 1.47 us
    pallas_call x1, Pallas kernels: 37.5 us -> 36.9 us  [fused_body(): pl.pallas_call(functools.partial(kernel, ep_size, tp_size, cap), out_shap...]
where the time goes in v2:
time: 38.6 us; the launch traced here: 38.4 us
  Pallas kernels  36.9 us (96%)
  local copies, waits for them, and re-layouts  1.47 us (4%)
    pallas_call x1, Pallas kernels, fused_body(): pl.pallas_call(functools.partial(kernel, ep_size, tp_size, cap), out_shap...  36.9 us
    unnamed x1, local copies, waits for them, and re-layouts  1.47 us

profile of v2, /device:TPU:0, one launch (start us, length us, event | category | flops | bytes accessed | tf_op | source)
XLA Modules:
  0.0 38.4 jit_solution(6595270690468196986)
XLA Ops:
  0.0 36.9 %shard_map.73 = bf16[256,128]{1,0:T(8,128)(2,1)} custom-call(bf16[32,1024]{1,0:T(8,128)(2,1)} %tok_h.1, f32[1,1024]{1,0:T(1,128)} %bitcast.7, s32[2,256]{1,0:T(2,128)} %bitcast.8, f32[2,256]{1,0:T(2,128)} %bitcast.9, bf16[2,32,1024]{2,1,0:T(8,128)(2,1)} %bitcast.5, bf16[2,32,1024]{2,1,0:T(8,128)(2,1)} %bitcast.6, bf16[2,32,1024]{2,1,0:T(8,128)(2,1)} %wd_h.1), custom_call_target="tpu_custom_call" | custom-call | tf_op jit(solution)/shard_map/pallas_call | solution.py:251
  36.9 1.5 %copy.9 = bf16[256,128]{1,0:T(8,128)(2,1)} copy(bf16[256,128]{1,0:T(8,128)(2,1)} %shard_map.73) | data formatting | bytes 131072

commit v3 on v2

--- a/solution.py
+++ b/solution.py
@@ -9,7 +9,7 @@
 
 epsilon = 1e-06
 MESH = pl.DeviceIdType.MESH
-CHUNKS = 4
+CHUNKS = 2
 
 
 def kernel(ep_size, tp_size, cap, tok_h, gain_h, routing_h, share_h, wg, wu, wd_h, out,
@@ -79,7 +79,7 @@
 
     pl.semaphore_wait(bar, tp_size - 1 + ep_size - 1)
 
-    zorder = [Z // 2] + [k for k in range(1, Z) if k != Z // 2]
+    zorder = [k for k in range(1, Z) if k != Z // 2] + [Z // 2]
     for c in range(CHUNKS):
         for k in zorder:
             start(rc(gblock(c, j), gblock(c, j), s1s.at[c, k], s1r.at[c, k], (g, zpeer(k))))

time: 38.6 us -> 36.2 us (0.938)
  Pallas kernels: 36.9 us -> 34.6 us
    pallas_call x1, Pallas kernels: 36.9 us -> 34.6 us  [fused_body(): pl.pallas_call(functools.partial(kernel, ep_size, tp_size, cap), out_shap...]
where the time goes in v3:
time: 36.2 us; the launch traced here: 36 us
  Pallas kernels  34.6 us (96%)
  local copies, waits for them, and re-layouts  1.47 us (4%)
    pallas_call x1, Pallas kernels, fused_body(): pl.pallas_call(functools.partial(kernel, ep_size, tp_size, cap), out_shap...  34.6 us
    unnamed x1, local copies, waits for them, and re-layouts  1.47 us

profile of v3, /device:TPU:0, one launch (start us, length us, event | category | flops | bytes accessed | tf_op | source)
XLA Modules:
  0.0 36.0 jit_solution(12894275739761074074)
XLA Ops:
  0.0 34.6 %shard_map.73 = bf16[256,128]{1,0:T(8,128)(2,1)} custom-call(bf16[32,1024]{1,0:T(8,128)(2,1)} %tok_h.1, f32[1,1024]{1,0:T(1,128)} %bitcast.7, s32[2,256]{1,0:T(2,128)} %bitcast.8, f32[2,256]{1,0:T(2,128)} %bitcast.9, bf16[2,32,1024]{2,1,0:T(8,128)(2,1)} %bitcast.5, bf16[2,32,1024]{2,1,0:T(8,128)(2,1)} %bitcast.6, bf16[2,32,1024]{2,1,0:T(8,128)(2,1)} %wd_h.1), custom_call_target="tpu_custom_call" | custom-call | tf_op jit(solution)/shard_map/pallas_call | solution.py:251
  34.6 1.5 %copy.9 = bf16[256,128]{1,0:T(8,128)(2,1)} copy(bf16[256,128]{1,0:T(8,128)(2,1)} %shard_map.73) | data formatting | bytes 131072
